TPU v7x, 32 devices: a whole 2x2x4 slice. The times are simulated.
32 devices in a mesh: fs: 4 (over z), rep: 2 (over y), tp: 4 (over x, core).
Axes of the slice: x: 2, y: 2, z: 4, core: 2. Of those that a mesh axis runs over, the one named last changes fastest.
Arguments:
- saved_input: bfloat16 [5120, 3072], P(('fs', 'rep')), may hold values from -6 to 6
- key_cotangent: bfloat16 [5120, 1024], P(('fs', 'rep'), 'tp'), may hold values from -0.0625 to 0.0625
- value_cotangent: bfloat16 [5120, 2048], P(('fs', 'rep'), 'tp'), may hold values from -0.0625 to 0.0625
- key_factor: bfloat16 [3072, 256], replicated, may hold values from -0.375 to 0.375
- value_factor: bfloat16 [3072, 256], replicated, may hold values from -0.375 to 0.375
- key_weight: float32 [3072, 1024], P(('fs', 'rep'), 'tp'), may hold values from -0.109375 to 0.109375
- value_weight: float32 [3072, 2048], P(('fs', 'rep'), 'tp'), may hold values from -0.109375 to 0.109375
- key_first: float32 [256, 1024], P(None, 'tp'), as said below
- key_second: float32 [256, 1024], P(None, 'tp'), may hold values from 0.05 to 1
- value_first: float32 [256, 2048], P(None, 'tp'), as said below
- value_second: float32 [256, 2048], P(None, 'tp'), may hold values from 0.05 to 1
Outputs:
- key_weight_new: float32 [3072, 1024], P(('fs', 'rep'), 'tp')
- value_weight_new: float32 [3072, 2048], P(('fs', 'rep'), 'tp')
- key_first_new: float32 [256, 1024], P(None, 'tp')
- key_second_new: float32 [256, 1024], P(None, 'tp')
- value_first_new: float32 [256, 2048], P(None, 'tp')
- value_second_new: float32 [256, 2048], P(None, 'tp')
- key_step: float32 [3072, 1024], P(('fs', 'rep'), 'tp')
- value_step: float32 [3072, 2048], P(('fs', 'rep'), 'tp')
- key_copy: bfloat16 [3072, 1024], P(None, 'tp')
- value_copy: bfloat16 [3072, 2048], P(None, 'tp')
Inputs may be any that keep to these rules, and one draw needn't show every extreme that they name: `key_first`: real-valued moments whose scale differs from head to head. `value_first`: real-valued moments whose scale differs from head to head.
All inputs are finite; a program needn't handle non-finite values.
Results may differ from a plain program's by a relative error of at most 0.004.
Values may be sent and summed in bfloat16 or wider, within the bound.
No kernel may reach another device: no remote copies, remote signals or barrier semaphores. Data moves between devices by JAX's collectives and lax.ppermute only.
A program may use at most 64 MiB of HBM per device.

v0:
```python
import jax
import jax.numpy as jnp
from jax import lax
from jax.sharding import PartitionSpec as P

DK = 1024
DV = 2048
RK = 256
RV = 256
first_decay = 0.8
second_decay = 0.9
epsilon = 1e-08
learn_rate = 0.01


def split_contract(basis, cotangent):
    upper = basis.astype(jnp.bfloat16)
    lower = (basis - upper.astype(jnp.float32)).astype(jnp.bfloat16)
    dims = (((0,), (0,)), ((), ()))
    high_part = lax.dot_general(upper, cotangent, dims, preferred_element_type=jnp.float32)
    low_part = lax.dot_general(lower, cotangent, dims, preferred_element_type=jnp.float32)
    return high_part + low_part


def moments(projection, first, second):
    first_new = first_decay * first + (1.0 - first_decay) * projection
    second_new = second_decay * second + (1.0 - second_decay) * projection * projection
    normed = first_new / (jnp.sqrt(second_new) + epsilon)
    return (first_new, second_new, normed)


def body(
    saved_input,
    key_cotangent,
    value_cotangent,
    key_factor,
    value_factor,
    key_weight,
    value_weight,
    key_first,
    key_second,
    value_first,
    value_second,
):
    local_rows = key_weight.shape[0]
    row_offset = lax.axis_index(("fs", "rep")) * local_rows
    key_rows = lax.dynamic_slice_in_dim(key_factor, row_offset, local_rows, 0).astype(jnp.float32)
    value_rows = lax.dynamic_slice_in_dim(value_factor, row_offset, local_rows, 0).astype(
        jnp.float32
    )
    key_basis = jnp.dot(saved_input, key_factor, preferred_element_type=jnp.float32)
    key_part = split_contract(key_basis, key_cotangent)
    value_basis = jnp.dot(saved_input, value_factor, preferred_element_type=jnp.float32)
    value_part = split_contract(value_basis, value_cotangent)
    key_projected, value_projected = lax.psum((key_part, value_part), ("fs", "rep"))
    key_first_new, key_second_new, key_normed = moments(key_projected, key_first, key_second)
    value_first_new, value_second_new, value_normed = moments(
        value_projected, value_first, value_second
    )
    local_squares = jnp.sum(key_normed * key_normed) + jnp.sum(value_normed * value_normed)
    squares = lax.psum(local_squares, "tp")
    entries = jnp.float32(RK * DK + RV * DV)
    shrink = jnp.sqrt(entries / (entries + squares))
    key_step = shrink * jnp.dot(key_rows, key_normed, precision=lax.Precision.HIGHEST)
    value_step = shrink * jnp.dot(value_rows, value_normed, precision=lax.Precision.HIGHEST)
    key_weight_new = key_weight - learn_rate * key_step
    value_weight_new = value_weight - learn_rate * value_step
    key_copy, value_copy = (
        lax.all_gather(key_weight_new.astype(jnp.bfloat16), ("fs", "rep"), axis=0, tiled=True),
        lax.all_gather(value_weight_new.astype(jnp.bfloat16), ("fs", "rep"), axis=0, tiled=True),
    )
    return (
        key_weight_new,
        value_weight_new,
        key_first_new,
        key_second_new,
        value_first_new,
        value_second_new,
        key_step,
        value_step,
        key_copy,
        value_copy,
    )


def solution(mesh):
    in_specs = (
        P(("fs", "rep"), None),
        P(("fs", "rep"), "tp"),
        P(("fs", "rep"), "tp"),
        P(),
        P(),
        P(("fs", "rep"), "tp"),
        P(("fs", "rep"), "tp"),
        P(None, "tp"),
        P(None, "tp"),
        P(None, "tp"),
        P(None, "tp"),
    )
    out_specs = (
        P(("fs", "rep"), "tp"),
        P(("fs", "rep"), "tp"),
        P(None, "tp"),
        P(None, "tp"),
        P(None, "tp"),
        P(None, "tp"),
        P(("fs", "rep"), "tp"),
        P(("fs", "rep"), "tp"),
        P(None, "tp"),
        P(None, "tp"),
    )
    return jax.shard_map(body, mesh=mesh, in_specs=in_specs, out_specs=out_specs, check_vma=False)
```

profile of v0, /device:TPU:0, one launch (start us, length us, event | category | flops | bytes accessed | tf_op | source)
XLA Modules:
  0.0 225.4 jit_solution(12211310105299718607)
XLA Ops:
  7.2 0.0 copy-start
  7.2 0.0 all-reduce.3.cloned.1.call-start
  7.2 1.3 copy-done
  8.6 3.4 %fusion.17 = f32[640,256]{1,0:T(8,128)S(1)} fusion(bf16[640,3072]{1,0:T(8,128)(2,1)} %param.11, bf16[3072,256]{1,0:T(8,128)(2,1)S(1)} %copy-done), kind=kOutput, calls=%fused_computation.31 | convolution fusion | flops 1006632960 | bytes 6160384 | tf_op jit(solution)/shard_map/dot_general | solution.py:53
  12.1 0.4 fusion.5
  12.5 0.0 copy-start.11
  12.5 1.2 convolution_add_fusion
  13.7 0.3 copy-done.11
  13.9 1.2 fusion.16
  15.1 0.0 copy-start.8
  15.2 0.3 fusion.8
  15.5 1.0 convolution_add_fusion.1
  16.5 0.0 all-reduce.3.cloned.1.call-update
  16.5 0.0 all-gather.3.cloned.1.call-start
  16.6 77.9 %all-reduce.3.cloned.1.call-done = (f32[256,256]{1,0:T(8,128)}, f32[256,512]{1,0:T(8,128)}) async-done(((f32[256,256]{1,0:T(8,128)}, f32[256,512]{1,0:T(8,128)}), (f32[256,256]{1,0:T(8,128)}, f32[256,512]{1,0:T(8,128)})) %all-reduce.3.cloned.1.call-update) | async-done | bytes 786448 | tf_op jit(solution)/shard_map/psum | solution.py:55
  94.5 0.0 copy-done.8
  94.5 2.2 multiply_reduce_fusion
  96.7 2.2 multiply_reduce_fusion.1
  100.2 6.2 %psum.23 = f32[]{:T(128)} all-reduce(f32[]{:T(128)S(6)} %add.59), channel_id=1, replica_groups=mesh['fs'=4,'rep'=2,'tp'=4] {'tp'}, use_global_device_ids=true, to_apply=%region_4.0 | all-reduce | flops 1 | bytes 8 | tf_op jit(solution)/shard_map/psum | solution.py:61
  107.1 2.3 %fusion.13 = (bf16[384,256]{1,0:T(8,128)(2,1)}, f32[384,256]{1,0:T(8,128)}, f32[384,256]{1,0:T(8,128)}) fusion(f32[384,256]{1,0:T(8,128)S(1)} %copy-done.9, f32[256,256]{1,0:T(8,128)S(1)} %get-tuple-element.36, f32[256,256]{1,0:T(8,128)S(1)} %get-tuple-element.37, bf16[3072,256]{1,0:T(8,128)(2,1)} %param.14, s32[]{:T(128)S(6)} %select_n.4, f32[]{:T(128)S(6)} %sqrt.11), kind=kOutput, calls=%fused_computation.29 | convolution fusion | flops 302514176 | bytes 2097160 | tf_op jit(solution)/shard_map/dot_general | solution.py:64
  109.4 0.0 all-gather.3.cloned.1.call-update
  109.5 0.0 all-gather.5.cloned.1.call-start
  109.5 0.0 copy-done.3
  109.5 0.0 copy-done.4
  109.5 3.2 %fusion.12 = (bf16[384,512]{1,0:T(8,128)(2,1)}, f32[384,512]{1,0:T(8,128)}, f32[384,512]{1,0:T(8,128)}) fusion(f32[384,512]{1,0:T(8,128)} %param.17, f32[256,512]{1,0:T(8,128)S(1)} %get-tuple-element.38, f32[256,512]{1,0:T(8,128)S(1)} %get-tuple-element.39, bf16[3072,256]{1,0:T(8,128)(2,1)S(1)} %copy-done, s32[]{:T(128)S(6)} %select_n.4, f32[]{:T(128)S(6)} %sqrt.11), kind=kOutput, calls=%fused_computation.28 | convolution fusion | flops 605028352 | bytes 3997704 | tf_op jit(solution)/shard_map/dot_general | solution.py:65
  112.7 0.0 copy-done.6
  112.7 0.0 all-gather.5.cloned.1.call-update
  112.7 40.5 %all-gather.3.cloned.1.call-done = bf16[3072,256]{1,0:T(8,128)(2,1)} async-done(((bf16[384,256]{1,0:T(8,128)(2,1)}), bf16[3072,256]{1,0:T(8,128)(2,1)}) %all-gather.3.cloned.1.call-update) | async-done | bytes 1572880 | tf_op jit(solution)/shard_map/all_gather | solution.py:69
  153.2 61.2 %all-gather.5.cloned.1.call-done = bf16[3072,512]{1,0:T(8,128)(2,1)} async-done(((bf16[384,512]{1,0:T(8,128)(2,1)}), bf16[3072,512]{1,0:T(8,128)(2,1)}) %all-gather.5.cloned.1.call-update) | async-done | bytes 3145744 | tf_op jit(solution)/shard_map/all_gather | solution.py:70
  214.4 2.8 %copy.25 = bf16[3072,256]{1,0:T(8,128)(2,1)} copy(bf16[3072,256]{1,0:T(8,128)(2,1)} %all-gather.3.cloned.1.call-done) | data formatting | bytes 3145728
  217.2 0.0 copy-done.1
  217.2 1.7 copy.26
  (16 shorter events, 0.0 us)
Async XLA Ops:
  7.2 1.4 copy-start
  7.2 4.9 %copy-start.2 = (bf16[640,512]{1,0:T(8,128)(2,1)S(1)}, bf16[640,512]{1,0:T(8,128)(2,1)}, u32[]{:S(2)}) copy-start(bf16[640,512]{1,0:T(8,128)(2,1)} %param.13) | copy-start | bytes 1966084
  7.2 87.3 %all-reduce.3.cloned.1.call-start = ((), (), s32[]{:S(2)}) async-start(), calls=%async_computation.2 | async-start | bytes 1572864 | tf_op jit(solution)/shard_map/psum | solution.py:55
  8.6 5.1 %copy-start.12 = (bf16[640,3072]{1,0:T(8,128)(2,1)S(1)}, bf16[640,3072]{1,0:T(8,128)(2,1)}, u32[]{:S(2)}) copy-start(bf16[640,3072]{1,0:T(8,128)(2,1)} %param.11) | copy-start | bytes 11796484
  12.5 1.5 copy-start.11
  13.9 1.2 copy-start.5
  15.1 79.4 %copy-start.8 = (f32[256,512]{1,0:T(8,128)S(1)}, f32[256,512]{1,0:T(8,128)}, u32[]{:S(2)}) copy-start(f32[256,512]{1,0:T(8,128)} %param.21) | copy-start | bytes 1572868
  16.5 136.7 %all-gather.3.cloned.1.call-start = ((), (), s32[]{:S(2)}) async-start(), calls=%async_computation | async-start | bytes 1769472 | tf_op jit(solution)/shard_map/all_gather | solution.py:69
  94.5 2.2 copy-start.10
  94.5 12.6 %copy-start.9 = (f32[384,256]{1,0:T(8,128)S(1)}, f32[384,256]{1,0:T(8,128)}, u32[]{:S(2)}) copy-start(f32[384,256]{1,0:T(8,128)} %param.16) | copy-start | bytes 1179652
  96.7 12.8 %copy-start.3 = (f32[256,512]{1,0:T(8,128)}, f32[256,512]{1,0:T(8,128)S(1)}, u32[]{:S(2)}) copy-start(f32[256,512]{1,0:T(8,128)S(1)} %get-tuple-element.39) | copy-start | bytes 1572868
  96.7 12.8 %copy-start.4 = (f32[256,512]{1,0:T(8,128)}, f32[256,512]{1,0:T(8,128)S(1)}, u32[]{:S(2)}) copy-start(f32[256,512]{1,0:T(8,128)S(1)} %get-tuple-element.38) | copy-start | bytes 1572868
  98.9 13.8 %copy-start.6 = (f32[256,256]{1,0:T(8,128)}, f32[256,256]{1,0:T(8,128)S(1)}, u32[]{:S(2)}) copy-start(f32[256,256]{1,0:T(8,128)S(1)} %get-tuple-element.37) | copy-start | bytes 786436
  98.9 13.8 %copy-start.7 = (f32[256,256]{1,0:T(8,128)}, f32[256,256]{1,0:T(8,128)S(1)}, u32[]{:S(2)}) copy-start(f32[256,256]{1,0:T(8,128)S(1)} %get-tuple-element.36) | copy-start | bytes 786436
  109.5 104.9 %all-gather.5.cloned.1.call-start = ((), (), s32[]{:S(2)}) async-start(), calls=%async_computation.1 | async-start | bytes 3538944 | tf_op jit(solution)/shard_map/all_gather | solution.py:70
  214.4 2.8 %copy-start.1 = (bf16[3072,512]{1,0:T(8,128)(2,1)S(1)}, bf16[3072,512]{1,0:T(8,128)(2,1)}, u32[]{:S(2)}) copy-start(bf16[3072,512]{1,0:T(8,128)(2,1)} %all-gather.5.cloned.1.call-done) | copy-start | bytes 9437188
Sparse Core Ops, SparseCore 0:
  16.6 77.8 all-reduce.2
  109.6 43.5 all-gather.2
  156.0 58.3 all-gather.4
where the time goes:
time: 226 us; the launch traced here: 225 us
  waiting for transfers between devices  180 us (80%)
  between operations  15.9 us (7%)
  matrix products  13 us (6%)
  blocking collectives  6.17 us (3%)
  local copies, waits for them, and re-layouts  6.12 us (3%)
  other arithmetic  4.39 us (2%)
    psum x1, waiting for transfers between devices, body(): lax.psum((key_part, value_part), ('fs', 'rep'))  77.9 us
    all_gather x1, waiting for transfers between devices, body(): lax.all_gather(value_weight_new.astype(jnp.bfloat16), ('fs', 'rep'), axis...  61.2 us
    all_gather x1, waiting for transfers between devices, body(): lax.all_gather(key_weight_new.astype(jnp.bfloat16), ('fs', 'rep'), axis=0...  40.5 us
    psum x1, blocking collectives, body(): squares = lax.psum(local_squares, 'tp')  6.17 us
    unnamed x28, local copies, waits for them, and re-layouts  6.12 us
  transfers between devices with their start and end apart: 3, of which 3 were waited for; matrix products, arithmetic and copies ran while one was open for 1% of the time, Pallas kernels for 0%

commit v1 on v0

--- a/solution.py
+++ b/solution.py
@@ -11,6 +11,18 @@
 second_decay = 0.9
 epsilon = 1e-08
 learn_rate = 0.01
+
+
+def gather_by_bits(shard, axis, dim):
+    ways, here = (lax.axis_size(axis), lax.axis_index(axis))
+    grown, reach = (shard, 1)
+    while reach < ways:
+        theirs = lax.ppermute(grown, axis, [(d, d ^ reach) for d in range(ways)])
+        mine_first = jnp.concatenate([grown, theirs], axis=dim)
+        theirs_first = jnp.concatenate([theirs, grown], axis=dim)
+        grown = jnp.where(here & reach == 0, mine_first, theirs_first)
+        reach = 2 * reach
+    return grown
 
 
 def split_contract(basis, cotangent):
@@ -67,7 +79,7 @@
     value_weight_new = value_weight - learn_rate * value_step
     key_copy, value_copy = (
         lax.all_gather(key_weight_new.astype(jnp.bfloat16), ("fs", "rep"), axis=0, tiled=True),
-        lax.all_gather(value_weight_new.astype(jnp.bfloat16), ("fs", "rep"), axis=0, tiled=True),
+        gather_by_bits(value_weight_new.astype(jnp.bfloat16), ("fs", "rep"), 0),
     )
     return (
         key_weight_new,

time: 226 us -> 238 us (1.053)
  waiting for transfers between devices: 180 us -> 187 us
  other arithmetic: 4.39 us -> 10.4 us
  local copies, waits for them, and re-layouts: 6.12 us -> 2.8 us
    ppermute x0 -> x3, waiting for transfers between devices: none -> 68.2 us  [gather_by_bits(): theirs = lax.ppermute(grown, axis, [(d, d ^ reach) for d in range(ways)])]
    all_gather x1 -> x0, waiting for transfers between devices: 61.2 us -> none  [body(): lax.all_gather(value_weight_new.astype(jnp.bfloat16), ('fs', 'rep'), axis...]
    select_n x0 -> x3, other arithmetic: none -> 6.01 us  [gather_by_bits(): grown = jnp.where(here & reach == 0, mine_first, theirs_first)]
    unnamed x28 -> x27, local copies, waits for them, and re-layouts: 6.12 us -> 2.8 us
  transfers between devices with their start and end apart: 3 -> 5, of which waited for: 3 -> 5; matrix products, arithmetic and copies ran while one was open for 1% -> 2% of each run, Pallas kernels for 0% -> 0%
where the time goes in v1:
time: 238 us
  waiting for transfers between devices  187 us (79%)
  between operations  16.2 us (7%)
  matrix products  13.1 us (6%)
  other arithmetic  10.4 us (4%)
  blocking collectives  6.17 us (3%)
  local copies, waits for them, and re-layouts  2.8 us (1%)
    psum x1, waiting for transfers between devices, body(): lax.psum((key_part, value_part), ('fs', 'rep'))  77.9 us
    ppermute x3, waiting for transfers between devices, gather_by_bits(): theirs = lax.ppermute(grown, axis, [(d, d ^ reach) for d in range(ways)])  68.2 us
    all_gather x1, waiting for transfers between devices, body(): lax.all_gather(key_weight_new.astype(jnp.bfloat16), ('fs', 'rep'), axis=0...  40.9 us
    psum x1, blocking collectives, body(): squares = lax.psum(local_squares, 'tp')  6.17 us
    select_n x3, other arithmetic, gather_by_bits(): grown = jnp.where(here & reach == 0, mine_first, theirs_first)  6.01 us
  transfers between devices with their start and end apart: 5, of which 5 were waited for; matrix products, arithmetic and copies ran while one was open for 2% of the time, Pallas kernels for 0%

profile of v1, /device:TPU:0, one launch (start us, length us, event | category | flops | bytes accessed | tf_op | source)
XLA Modules:
  0.0 237.7 jit_solution(7876751817787351936)
XLA Ops:
  7.2 0.0 copy-start
  7.2 0.0 all-reduce.3.cloned.1.call-start
  7.2 1.3 copy-done
  8.6 3.4 %fusion.17 = f32[640,256]{1,0:T(8,128)S(1)} fusion(bf16[640,3072]{1,0:T(8,128)(2,1)} %param.11, bf16[3072,256]{1,0:T(8,128)(2,1)S(1)} %copy-done), kind=kOutput, calls=%fused_computation.34 | convolution fusion | flops 1006632960 | bytes 6160384 | tf_op jit(solution)/shard_map/dot_general | solution.py:65
  12.1 0.4 fusion.5
  12.5 0.0 copy-start.11
  12.5 1.2 convolution_add_fusion
  13.7 0.3 copy-done.11
  13.9 1.2 fusion.16
  15.2 0.3 fusion.8
  15.5 1.0 convolution_add_fusion.1
  16.5 0.0 all-reduce.3.cloned.1.call-update
  16.5 0.0 all-gather.2.cloned.1.call-start
  16.6 77.9 %all-reduce.3.cloned.1.call-done = (f32[256,256]{1,0:T(8,128)}, f32[256,512]{1,0:T(8,128)}) async-done(((f32[256,256]{1,0:T(8,128)}, f32[256,512]{1,0:T(8,128)}), (f32[256,256]{1,0:T(8,128)}, f32[256,512]{1,0:T(8,128)})) %all-reduce.3.cloned.1.call-update) | async-done | bytes 786448 | tf_op jit(solution)/shard_map/psum | solution.py:67
  94.5 2.2 multiply_reduce_fusion
  96.7 2.2 multiply_reduce_fusion.1
  100.2 6.2 %psum.23 = f32[]{:T(128)} all-reduce(f32[]{:T(128)S(6)} %add.60), channel_id=1, replica_groups=mesh['fs'=4,'rep'=2,'tp'=4] {'tp'}, use_global_device_ids=true, to_apply=%region_4.0 | all-reduce | flops 1 | bytes 8 | tf_op jit(solution)/shard_map/psum | solution.py:73
  107.1 3.0 %fusion.12 = (bf16[384,512]{1,0:T(8,128)(2,1)S(1)}, f32[384,512]{1,0:T(8,128)}, f32[384,512]{1,0:T(8,128)}) fusion(f32[384,512]{1,0:T(8,128)} %param.17, f32[256,512]{1,0:T(8,128)S(1)} %get-tuple-element.38, f32[256,512]{1,0:T(8,128)S(1)} %get-tuple-element.39, bf16[3072,256]{1,0:T(8,128)(2,1)S(1)} %copy-done, s32[]{:T(128)S(6)} %select_n.28, f32[]{:T(128)S(6)} %sqrt.11), kind=kOutput, calls=%fused_computation.31 | convolution fusion | flops 605028352 | bytes 3997704 | tf_op jit(solution)/shard_map/dot_general | solution.py:77
  110.1 0.8 collective-permute-start
  110.9 2.5 %fusion.13 = (bf16[384,256]{1,0:T(8,128)(2,1)}, f32[384,256]{1,0:T(8,128)}, f32[384,256]{1,0:T(8,128)}) fusion(f32[384,256]{1,0:T(8,128)} %param.16, f32[256,256]{1,0:T(8,128)S(1)} %get-tuple-element.36, f32[256,256]{1,0:T(8,128)S(1)} %get-tuple-element.37, bf16[3072,256]{1,0:T(8,128)(2,1)} %param.14, s32[]{:T(128)S(6)} %select_n.28, f32[]{:T(128)S(6)} %sqrt.11), kind=kOutput, calls=%fused_computation.32 | convolution fusion | flops 302514176 | bytes 2097160 | tf_op jit(solution)/shard_map/dot_general | solution.py:76
  113.4 0.0 all-gather.2.cloned.1.call-update
  113.4 7.6 %collective-permute-done = bf16[384,512]{1,0:T(8,128)(2,1)S(1)} collective-permute-done((bf16[384,512]{1,0:T(8,128)(2,1)S(1)}, bf16[384,512]{1,0:T(8,128)(2,1)S(1)}, u32[]{:S(2)}, u32[]{:S(2)}) %collective-permute-start) | collective-permute-done | bytes 393248 | tf_op jit(solution)/shard_map/ppermute | solution.py:20
  121.0 0.3 maximum_select_fusion.2
  121.3 0.0 copy-start.1
  121.3 1.0 collective-permute-start.1
  122.4 30.3 %collective-permute-done.1 = bf16[768,512]{1,0:T(8,128)(2,1)} collective-permute-done((bf16[768,512]{1,0:T(8,128)(2,1)S(1)}, bf16[768,512]{1,0:T(8,128)(2,1)}, u32[]{:S(2)}, u32[]{:S(2)}) %collective-permute-start.1) | collective-permute-done | bytes 786464 | tf_op jit(solution)/shard_map/ppermute | solution.py:20
  152.7 2.3 maximum_select_fusion.1
  155.0 0.1 collective-permute-start.2
  155.1 40.9 %all-gather.2.cloned.1.call-done = bf16[3072,256]{1,0:T(8,128)(2,1)} async-done(((bf16[384,256]{1,0:T(8,128)(2,1)}), bf16[3072,256]{1,0:T(8,128)(2,1)}) %all-gather.2.cloned.1.call-update) | async-done | bytes 1572880 | tf_op jit(solution)/shard_map/all_gather | solution.py:81
  196.0 30.3 %collective-permute-done.2 = bf16[1536,512]{1,0:T(8,128)(2,1)} collective-permute-done((bf16[1536,512]{1,0:T(8,128)(2,1)S(1)}, bf16[1536,512]{1,0:T(8,128)(2,1)}, u32[]{:S(2)}, u32[]{:S(2)}) %collective-permute-start.2) | collective-permute-done | bytes 1572896 | tf_op jit(solution)/shard_map/ppermute | solution.py:20
  226.3 3.4 %maximum_select_fusion = bf16[3072,512]{1,0:T(8,128)(2,1)} fusion(bf16[1536,512]{1,0:T(8,128)(2,1)} %collective-permute-done.2, bf16[1536,512]{1,0:T(8,128)(2,1)S(1)} %maximum_select_fusion.1, pred[]{:T(512)S(6)} %eq.9), kind=kLoop, calls=%fused_computation | loop fusion | flops 14155776 | bytes 6291457 | tf_op jit(solution)/shard_map/jit(_where)/select_n | solution.py:23
  229.7 1.1 copy.24
  (21 shorter events, 0.0 us)
Async XLA Ops:
  7.2 1.4 copy-start
  7.2 4.9 %copy-start.2 = (bf16[640,512]{1,0:T(8,128)(2,1)S(1)}, bf16[640,512]{1,0:T(8,128)(2,1)}, u32[]{:S(2)}) copy-start(bf16[640,512]{1,0:T(8,128)(2,1)} %param.13) | copy-start | bytes 1966084
  7.2 87.3 %all-reduce.3.cloned.1.call-start = ((), (), s32[]{:S(2)}) async-start(), calls=%async_computation.1 | async-start | bytes 1572864 | tf_op jit(solution)/shard_map/psum | solution.py:67
  8.6 5.1 %copy-start.12 = (bf16[640,3072]{1,0:T(8,128)(2,1)S(1)}, bf16[640,3072]{1,0:T(8,128)(2,1)}, u32[]{:S(2)}) copy-start(bf16[640,3072]{1,0:T(8,128)(2,1)} %param.11) | copy-start | bytes 11796484
  12.5 1.5 copy-start.11
  13.9 1.2 copy-start.6
  15.1 79.4 %copy-start.9 = (f32[256,512]{1,0:T(8,128)S(1)}, f32[256,512]{1,0:T(8,128)}, u32[]{:S(2)}) copy-start(f32[256,512]{1,0:T(8,128)} %param.21) | copy-start | bytes 1572868
  16.5 179.5 %all-gather.2.cloned.1.call-start = ((), (), s32[]{:S(2)}) async-start(), calls=%async_computation | async-start | bytes 1769472 | tf_op jit(solution)/shard_map/all_gather | solution.py:81
  94.5 2.2 copy-start.10
  96.7 13.4 %copy-start.3 = (f32[256,512]{1,0:T(8,128)}, f32[256,512]{1,0:T(8,128)S(1)}, u32[]{:S(2)}) copy-start(f32[256,512]{1,0:T(8,128)S(1)} %get-tuple-element.39) | copy-start | bytes 1572868
  96.7 13.4 %copy-start.4 = (f32[256,512]{1,0:T(8,128)}, f32[256,512]{1,0:T(8,128)S(1)}, u32[]{:S(2)}) copy-start(f32[256,512]{1,0:T(8,128)S(1)} %get-tuple-element.38) | copy-start | bytes 1572868
  98.9 12.1 %copy-start.7 = (f32[256,256]{1,0:T(8,128)}, f32[256,256]{1,0:T(8,128)S(1)}, u32[]{:S(2)}) copy-start(f32[256,256]{1,0:T(8,128)S(1)} %get-tuple-element.37) | copy-start | bytes 786436
  98.9 12.1 %copy-start.8 = (f32[256,256]{1,0:T(8,128)}, f32[256,256]{1,0:T(8,128)S(1)}, u32[]{:S(2)}) copy-start(f32[256,256]{1,0:T(8,128)S(1)} %get-tuple-element.36) | copy-start | bytes 786436
  110.1 10.9 %collective-permute-start = (bf16[384,512]{1,0:T(8,128)(2,1)S(1)}, bf16[384,512]{1,0:T(8,128)(2,1)S(1)}, u32[]{:S(2)}, u32[]{:S(2)}) collective-permute-start(bf16[384,512]{1,0:T(8,128)(2,1)S(1)} %get-tuple-element.12), channel_id=1, source_target_pairs={{0,4},{4,0},{8,12},{12,8},{16,20},{20,16},{24,28},{28,24},{1,5},{5... | collective-permute-start | bytes 1179656 | tf_op jit(solution)/shard_map/ppermute | solution.py:20
  121.3 1.1 copy-start.1
  121.3 31.4 %collective-permute-start.1 = (bf16[768,512]{1,0:T(8,128)(2,1)S(1)}, bf16[768,512]{1,0:T(8,128)(2,1)}, u32[]{:S(2)}, u32[]{:S(2)}) collective-permute-start(bf16[768,512]{1,0:T(8,128)(2,1)S(1)} %maximum_select_fusion.2), channel_id=1, source_target_pairs={{0,8},{4,12},{8,0},{12,4},{16,24},{20,28},{24,16},{28,20},{1,9},{5... | collective-permute-start | bytes 2359304 | tf_op jit(solution)/shard_map/ppermute | solution.py:20
  155.0 71.3 %collective-permute-start.2 = (bf16[1536,512]{1,0:T(8,128)(2,1)S(1)}, bf16[1536,512]{1,0:T(8,128)(2,1)}, u32[]{:S(2)}, u32[]{:S(2)}) collective-permute-start(bf16[1536,512]{1,0:T(8,128)(2,1)S(1)} %maximum_select_fusion.1), channel_id=1, source_target_pairs={{0,16},{4,20},{8,24},{12,28},{16,0},{20,4},{24,8},{28,12},{1,17},{... | collective-permute-start | bytes 4718600 | tf_op jit(solution)/shard_map/ppermute | solution.py:20
  196.0 33.7 %copy-start.5 = (bf16[3072,256]{1,0:T(8,128)(2,1)S(1)}, bf16[3072,256]{1,0:T(8,128)(2,1)}, u32[]{:S(2)}) copy-start(bf16[3072,256]{1,0:T(8,128)(2,1)} %all-gather.2.cloned.1.call-done) | copy-start | bytes 4718596
Sparse Core Ops, SparseCore 0:
  16.6 77.8 all-reduce.2
  113.6 82.3 all-gather.1
